TPU v7x, 128 devices: a whole 4x4x4 slice. The times are simulated.
128 devices in a mesh: tp: 16 (over z, y), dp: 8 (over x, core).
Axes of the slice: x: 4, y: 4, z: 4, core: 2. Of those that a mesh axis runs over, the one named last changes fastest.
Arguments:
- activation_rows: bfloat16 [2048, 4096], P(None, 'dp'), may hold values from -24 to 24
- fresh_spans: int32 [256], P('dp'), may hold values from 1 to 8, 768 in all
- entry_rescale_vector: float32 [2, 4096], P(None, 'dp'), may hold values from 0.1 to 1.9
- probe_kernel: bfloat16 [2, 4096, 4096], P(None, 'dp', 'tp'), may hold values from -0.09375 to 0.09375
- retention_kernel: bfloat16 [2, 4096, 4096], P(None, 'dp', 'tp'), may hold values from -0.09375 to 0.09375
- content_kernel: bfloat16 [2, 4096, 4096], P(None, 'dp', 'tp'), may hold values from -0.09375 to 0.09375
- valve_kernel: bfloat16 [2, 4096, 4096], P(None, 'dp', 'tp'), may hold values from -0.09375 to 0.09375
- retention_minimum: float32 [2, 4096], P(None, 'tp'), may hold values from 0 to 0.99
- extra_attenuation: float32 [2, 2048, 32], P(None, 'dp', 'tp'), may hold values from -0.7 to 0
- channel_rescale_vector: float32 [2, 4096], P(None, 'tp'), may hold values from 0.1 to 1.9
- emission_kernel: bfloat16 [2, 4096, 4096], P(None, 'tp', 'dp'), may hold values from -0.09375 to 0.09375
- memory_grids: float32 [2, 256, 32, 128, 128], P(None, 'dp', 'tp'), may hold values from -0.6 to 0.6
Outputs:
- mixed: bfloat16 [2048, 4096], P(None, 'dp')
- new_states: float32 [2, 256, 32, 128, 128], P(None, 'dp', 'tp')
Inputs may be any that keep to these rules, and one draw needn't show every extreme that they name: `fresh_spans`: each sequence has at least one live slot.
All inputs are finite; a program needn't handle non-finite values. No bound on the sum of `fresh_spans` on one device may be relied on, other than what follows from the above.
Results may differ from a plain program's by a relative error of at most 0.017.
Values may be sent and summed in bfloat16 or wider, within the bound.
A program may use at most 128 MiB of HBM per device.

v0:
```python
import functools

import jax
import jax.numpy as jnp
from jax import lax
from jax.experimental import pallas as pl
from jax.experimental.pallas import tpu as pltpu
from jax.sharding import PartitionSpec as P

D = 4096
BLOCKS = 2
EPSILON = 1e-05
RING = 4
SHARDS = 8
SEQS = 32
SLOTS = 8
SHARD_ROWS = SEQS * SLOTS
FEATURES = 512
CHANNELS = 256
HEADS = 2
LANES = 128
MESH = pl.DeviceIdType.MESH
F32 = jnp.float32
BF16 = jnp.bfloat16
CHUNKS = 2
ADVANCES = {(2, False): 3, (2, True): 1, (3, False): 1, (3, True): 1, (4, False): 1, (4, True): 1}
WIDE = FEATURES // CHUNKS
MIB = 1024 * 1024


def here():
    dp, tp = lax.axis_index("dp"), lax.axis_index("tp")
    return lax.div(dp, 2), lax.rem(dp, 2), lax.div(tp, RING), lax.rem(tp, RING)


def device(x, core, z, y):
    return {"tp": z * RING + y, "dp": x * 2 + core}


def around(index, offset):
    return lax.rem(index + offset, RING)


def greet(peers):
    barrier = pltpu.get_barrier_semaphore()
    for peer in peers:
        pl.semaphore_signal(barrier, inc=1, device_id=peer, device_id_type=MESH)
    pl.semaphore_wait(barrier, len(peers))


def iota(shape, dim):
    return lax.broadcasted_iota(jnp.int32, shape, dim)


def dot(a, b):
    return jnp.dot(a, b, preferred_element_type=F32)


def dot_rows(a, b):
    return lax.dot_general(a, b, (((0,), (0,)), ((), ())), preferred_element_type=F32)


def chosen(rank_row, first, count):
    wanted = (iota((count, rank_row.shape[1]), 0) + first).astype(F32)
    return jnp.where(wanted == rank_row, 1.0, 0.0).astype(BF16)


def fill_columns(spans, column):
    own = spans[...].astype(F32)
    lane, row = iota((SEQS, SEQS), 1), iota((SEQS, SEQS), 0)
    before = jnp.sum(jnp.where(lane < row, own, 0.0), axis=1, keepdims=True)
    same = jnp.sum(jnp.where(lane == row, own, 0.0), axis=1, keepdims=True)
    column[0:SEQS, :] = jnp.broadcast_to(before, (SEQS, LANES))
    column[SEQS:, :] = jnp.broadcast_to(same, (SEQS, LANES))


def fill_ranks(gathered, rank, many):
    spans_all = jnp.concatenate([gathered[index] for index in range(SHARDS)], axis=0).astype(F32)
    most = jnp.max(jnp.sum(spans_all, axis=1, keepdims=True))
    many[0, 0] = jnp.where(most > CAPACITY, 1, 0)
    spans_all = spans_all.astype(BF16)
    slot_index = iota((SEQS, SHARD_ROWS), 1)
    sequence = iota((SEQS, SHARD_ROWS), 0)
    for order in range(2):
        if order == 0:
            owner, position = lax.shift_right_logical(slot_index, 3), slot_index & 7
        else:
            owner, position = slot_index & 31, lax.shift_right_logical(slot_index, 5)
        earlier = jnp.where(sequence < owner, 1.0, 0.0).astype(BF16)
        equal = jnp.where(sequence == owner, 1.0, 0.0).astype(BF16)
        start, length = dot(spans_all, earlier), dot(spans_all, equal)
        place = position[0:SHARDS].astype(F32)
        ranks = jnp.where(place < length, start + place, -1.0)
        for index in range(SHARDS):
            rank[order * SHARDS + index] = ranks[index : index + 1]


def silu(a):
    return a * jax.nn.sigmoid(a)


def gates(b, head, lo, hi, refs):
    spread, column, minimum, added, q_decayed, own_read, keys, decay_total = refs
    ones = jnp.ones((LANES, LANES), BF16)
    low, high = head * LANES, (head + 1) * LANES
    done = lo // SLOTS // 8
    together = 2 if (SEQS // 8 - done) % 2 == 0 else 3

    def group(pair, carry):
        for unit in range(together):
            g = done + pair * together + unit
            start = column[pl.ds(pl.multiple_of(g * 8, 8), 8), :]
            span = column[pl.ds(pl.multiple_of(SEQS + g * 8, 8), 8), :]
            floor = minimum[b : b + 1, low:high]
            kept, values, products = [], [], []
            running = None
            for p in range(SLOTS):
                rows = pl.ds(pl.multiple_of(p * SEQS + g * 8, 8), 8)
                q = silu(spread[b, head, 0, rows, :])
                f = spread[b, head, 1, rows, :]
                values.append(spread[b, head, 2, rows, :])
                small = jnp.exp(-jnp.abs(f))
                large = 1.0 / (1.0 + small)
                small = small * large
                up = f >= 0.0
                live = jnp.logical_and(span > p, start + p < hi)
                forget = floor + (1.0 - floor) * jnp.where(up, large, small)
                decay = jnp.where(live, forget * added[b, head, pl.ds(g * 64 + p, 8, stride=8), :], 1.0)
                key = jnp.where(live, (1.0 - floor) * jnp.where(up, small, large), 0.0)
                running = decay if p == 0 else running * decay
                kept = [old * decay for old in kept] + [key]
                products += [q * old for old in kept]
                q_decayed[head, rows, :] = q * running
            for p in range(SLOTS):
                rows = pl.ds(pl.multiple_of(p * SEQS + g * 8, 8), 8)
                keys[b, head, rows, :] = kept[p]
            decay_total[b, pl.ds(pl.multiple_of(g * 8, 8), 8), low:high] = running
            scores = dot(jnp.concatenate(products, axis=0).astype(BF16), ones)
            number = 0
            for p in range(SLOTS):
                read = None
                for value in values[: p + 1]:
                    term = scores[number * 8 : (number + 1) * 8] * value
                    read = term if read is None else read + term
                    number += 1
                own_read[head, pl.ds(pl.multiple_of(p * SEQS + g * 8, 8), 8), :] = read
        return carry

    lax.fori_loop(0, (SEQS // 8 - done) // together, group, 0)


def reads(b, head, lo, refs):
    spread, rounded, gain, q_decayed, own_read, heads_out = refs
    together = 8
    low, high = head * LANES, (head + 1) * LANES

    def group(g, carry):
        for unit in range(together):
            s = g * together + unit
            rows = pl.ds(s, SLOTS, stride=SEQS)
            read = dot(q_decayed[head, rows, :].astype(BF16), rounded[s, head])
            read = read + own_read[head, rows, :]
            square = jnp.mean(read * read, axis=1, keepdims=True)
            gate = silu(spread[b, head, 3, rows, :])
            out = read * lax.rsqrt(square + EPSILON) * gain[b : b + 1, low:high] * gate
            heads_out[head, pl.ds(pl.multiple_of(s * SLOTS, SLOTS), SLOTS), :] = out
        return carry

    lax.fori_loop(lo // SLOTS // together, SEQS // together, group, 0)


def round_states(b, states, rounded):
    def group(g, carry):
        rounded[pl.ds(g * 4, 4)] = states[b, pl.ds(g * 4, 4)].astype(BF16)
        return carry

    lax.fori_loop(0, SEQS // 4, group, 0)


def advance_states(b, first, number, refs):
    states, spread, keys, decay_total = refs

    def group(g, carry):
        diagonal = iota((LANES, LANES), 0) == iota((LANES, LANES), 1)
        totals = decay_total[b, pl.ds(pl.multiple_of(g * 8, 8), 8), :]
        for unit in range(8):
            s = g * 8 + unit
            slots = pl.ds(s, SLOTS, stride=SEQS)
            for head in range(HEADS):
                added = dot_rows(
                    keys[b, head, slots, :].astype(BF16), spread[b, head, 2, slots, :].astype(BF16)
                )
                total = totals[unit : unit + 1, head * LANES : (head + 1) * LANES]
                kept = jnp.sum(jnp.where(diagonal, total, 0.0), axis=1, keepdims=True)
                states[b, s, head] = kept * states[b, s, head] + added
        return carry

    lax.fori_loop(first, first + number, group, 0)


def blocks_kernel(pieces, *refs):
    count = len(pieces)
    (spans, act, gain_in, w_q, w_f, w_v, w_g, minimum, extra, gain_out, emission, memory) = refs[:12]
    (rank, many, final_x, states) = refs[12:16]
    refs = list(refs[16:])

    def take(number):
        taken = refs[:number]
        del refs[:number]
        return taken

    (gathered, column, raw, gain_peer, weights, outward, rounded, normed, spread, q_decayed, own_read) = take(11)
    (heads_out, added, keys, decay_total) = take(4)
    (local_sems, swap_send, swap_recv, count_send, count_recv, send_sems, recv_sems) = take(7)
    per = [take(13) for _ in range(count)]
    x, core, z, y = here()
    dp = x * 2 + core

    xs = [device(around(x, o), core, z, y) for o in range(1, RING)]
    ys = [device(x, core, z, around(y, o)) for o in range(1, RING)]
    zs = [device(x, core, around(z, o), y) for o in range(1, RING)]
    crossed = [device(x, 1 - core, around(z, o), y) for o in range(RING)]
    others = [device(around(x, o), 1 - core, z, y) for o in range(1, RING)]
    partner = crossed[0]
    kernels = (w_q, w_f, w_v, w_g)

    local, swaps, sent = [], [], []

    def bring(source, target):
        copy = pltpu.make_async_copy(source, target, local_sems.at[len(local)])
        copy.start()
        local.append(copy)
        return copy

    def swap(source, target):
        number = len(swaps)
        copy = pltpu.make_async_remote_copy(
            source,
            target,
            swap_send.at[number],
            swap_recv.at[number],
            device_id=partner,
            device_id_type=MESH,
        )
        copy.start()
        swaps.append(copy)
        return copy

    def send(b, i, phase, number, source, target, peer):
        copy = pltpu.make_async_remote_copy(
            source,
            target,
            send_sems.at[b, i, phase, number],
            recv_sems.at[b, i, phase, number],
            device_id=peer,
            device_id_type=MESH,
        )
        copy.start()
        sent.append(copy)
        return copy

    def rows_of(side, j):
        return act.at[pl.ds((j * 2 + side) * SHARD_ROWS, SHARD_ROWS), :]

    def weight_parts(b, head, first):
        for k in range(4):
            yield (
                kernels[k].at[b, :, head * LANES : (head + 1) * LANES],
                weights.at[b, head, first : first + FEATURES, k * LANES : (k + 1) * LANES],
            )

    own_rows = [bring(rows_of(core, j), raw.at[j, :, 0:FEATURES]) for j in range(RING)]
    own_weights = [[[bring(*part) for part in weight_parts(0, h, 0)] for h in range(HEADS)]]
    own_states = [bring(memory.at[b], states.at[b]) for b in range(BLOCKS)]
    own_outward = [bring(emission.at[b], outward.at[b, :, 0:FEATURES]) for b in range(BLOCKS)]
    own_weights.append([[bring(*part) for part in weight_parts(1, h, 0)] for h in range(HEADS)])

    greet(xs + ys + zs + crossed + others)

    counts = []
    for number, peer in enumerate(xs + [partner] + others):
        copy = pltpu.make_async_remote_copy(
            spans,
            gathered.at[dp],
            count_send.at[number],
            count_recv.at[number],
            device_id=peer,
            device_id_type=MESH,
        )
        copy.start()
        counts.append(copy)
    peer_rows = [swap(rows_of(1 - core, j), raw.at[j, :, FEATURES : 2 * FEATURES]) for j in range(RING)]
    peer_gain = swap(gain_in, gain_peer)
    peer_weights = [[[swap(*part) for part in weight_parts(0, h, FEATURES)] for h in range(HEADS)]]
    peer_outward = [swap(emission.at[b], outward.at[b, :, FEATURES : 2 * FEATURES]) for b in range(BLOCKS)]
    peer_weights.append([[swap(*part) for part in weight_parts(1, h, FEATURES)] for h in range(HEADS)])

    gathered[dp] = spans[...]
    fill_columns(spans, column)
    for copy in counts:
        copy.wait_recv()
    fill_ranks(gathered, rank, many)
    for j in range(RING):
        own_rows[j].wait()
        peer_rows[j].wait_recv()
    peer_gain.wait_recv()
    waiting = []

    def widen():
        diagonal = iota((LANES, LANES), 0) == iota((LANES, LANES), 1)
        for b in range(BLOCKS):
            for head in range(HEADS):
                for part in range(SHARD_ROWS // LANES):
                    row = extra[b, head : head + 1, part * LANES : (part + 1) * LANES]
                    wide = jnp.sum(jnp.where(diagonal, jnp.exp(row), 0.0), axis=1, keepdims=True)
                    added[b, head, part * LANES : (part + 1) * LANES, :] = jnp.broadcast_to(wide, (LANES, LANES))

    def piece_steps(i):
        first, rows = pieces[i]
        (x_own, x_peer, parts, got, squares, got_squares, heads, u_own, u_peer, one, two_own, two_peer, last_peer) = per[i]
        for j in range(RING):
            picked = dot(chosen(rank[j * 2 + core], first, rows), raw[j]).astype(BF16)
            for part in range(CHUNKS):
                x_own[0, j, part] = picked[:, part * WIDE : (part + 1) * WIDE]
                x_peer[0, j, part] = picked[:, FEATURES + part * WIDE : FEATURES + (part + 1) * WIDE]
        for b in range(BLOCKS):
            wide = max(rows, LANES)
            eye = iota((rows, wide), 0) == iota((rows, wide), 1)
            for j in range(RING):
                at = slice(j * rows, (j + 1) * rows)
                for part in range(CHUNKS):
                    low, high = part * WIDE, (part + 1) * WIDE
                    own = x_own[b, j, part].astype(F32) * gain_in[b : b + 1, low:high]
                    peer = x_peer[b, j, part].astype(F32) * gain_peer[b : b + 1, low:high]
                    normed[at, low:high] = own.astype(BF16)
                    normed[at, FEATURES + low : FEATURES + high] = peer.astype(BF16)
            waits = []
            for head in range(HEADS):
                if i == 0:
                    for k in range(4):
                        own_weights[b][head][k].wait()
                        peer_weights[b][head][k].wait_recv()

                def project(k, carry, b=b, head=head):
                    columns = pl.ds(pl.multiple_of(k * CHANNELS, CHANNELS), CHANNELS)
                    product = dot(normed[0 : RING * rows], weights[b, head, :, columns]).astype(BF16)
                    for j in range(RING):
                        parts[b, head, j, :, columns] = product[j * rows : (j + 1) * rows]
                    return carry

                lax.fori_loop(0, 2, project, 0)
                for o in (2, 1, 3):
                    waits.append(
                        send(
                            b, i, 0, head * RING + o, parts.at[b, head, around(x, o)], got.at[b, head, o - 1], xs[o - 1]
                        )
                    )
            for j in range(RING):
                total = jnp.zeros((rows, 1), F32)
                for part in range(CHUNKS):
                    own = x_own[b, j, part].astype(F32)
                    peer = x_peer[b, j, part].astype(F32)
                    total = total + jnp.sum(own * own + peer * peer, axis=1, keepdims=True)
                squares[b, j] = jnp.sum(jnp.where(eye, total, 0.0), axis=0, keepdims=True)
            square_waits = []
            for o in (2, 1, 3):
                square_waits.append(
                    send(b, i, 1, o, squares.at[b, around(x, o)], got_squares.at[b, o - 1], xs[o - 1])
                )
            if i == count - 1:
                if b == 0:
                    widen()
                own_states[b].wait()
                round_states(b, states, rounded)
            yield

            for wait in square_waits:
                wait.wait_recv()
            square = squares[b, x] + got_squares[b, 0] + got_squares[b, 1] + got_squares[b, 2]
            scale_row = lax.rsqrt(square / D + EPSILON)
            scale = jnp.sum(jnp.where(eye, scale_row, 0.0), axis=1, keepdims=True)
            places = chosen(rank[SHARDS + dp], first, rows)
            picking = chosen(rank[dp], first, rows)
            head_waits = []
            for head in range(HEADS):
                for wait in waits[head * 3 : head * 3 + 3]:
                    wait.wait_recv()

                for part in range(2):
                    columns = slice(part * CHANNELS, (part + 1) * CHANNELS)
                    total = parts[b, head, x, :, columns].astype(F32)
                    for o in range(RING - 1):
                        total = total + got[b, head, o, :, columns].astype(F32)
                    placed = dot_rows(places, (total * scale).astype(BF16))
                    for k in range(2):
                        piece = placed[:, k * LANES : (k + 1) * LANES]
                        if i > 0:
                            piece = piece + spread[b, head, part * 2 + k]
                        spread[b, head, part * 2 + k] = piece
                gates(b, head, first, first + rows, (spread, column, minimum, added, q_decayed, own_read, keys, decay_total))
                reads(b, head, first, (spread, rounded, gain_out, q_decayed, own_read, heads_out))
                heads[b, head, x] = dot(picking, heads_out[head].astype(BF16)).astype(BF16)
                for o in (2, 1, 3):
                    mine = heads.at[b, head, x]
                    head_waits.append(send(b, i, 2, head * RING + o, mine, mine, xs[o - 1]))
            if i == count - 1:
                for g in range(SEQS // 8):
                    waiting.append(
                        functools.partial(advance_states, b, g, 1, (states, spread, keys, decay_total))
                    )
            if i == 0:
                own_outward[b].wait()
                peer_outward[b].wait_recv()
            yield

            for wait in head_waits:
                wait.wait_recv()
            all_heads = jnp.concatenate([heads[b, head].reshape(RING * rows, LANES) for head in range(HEADS)], axis=1)
            waits = []
            for part in range(CHUNKS):
                for half, (target, at, peers) in enumerate(((u_own, y, ys), (u_peer, z, zs))):
                    low = half * FEATURES + part * WIDE
                    product = dot(all_heads, outward[b, :, low : low + WIDE]).astype(BF16)
                    for j in range(RING):
                        target[b, j, part] = product[j * rows : (j + 1) * rows]
                    for o in (2, 1, 3):
                        waits.append(
                            send(
                                b, i, 3 + half, part * RING + o, target.at[b, around(at, o), part],
                                one.at[b, half, o - 1, part], peers[o - 1],
                            )
                        )
            yield

            later = []
            for part in range(CHUNKS):
                for half, (mine, at, slots, own, peers) in enumerate(
                    ((u_own, y, two_own, z, zs), (u_peer, z, two_peer, y, ys))
                ):
                    for wait in waits[:3]:
                        wait.wait_recv()
                    del waits[:3]
                    total = mine[b, at, part].astype(F32)
                    for o in range(RING - 1):
                        total = total + one[b, half, o, part].astype(F32)
                    slots[b, own, part] = total.astype(BF16)
                    place = slots.at[b, own, part]
                    for o in (2, 1, 3):
                        later.append(send(b, i, 5 + half, part * RING + o, place, place, peers[o - 1]))
            waits = later
            yield

            later = []
            for part in range(CHUNKS):
                for half, (slots, old, at) in enumerate(((two_own, x_own, y), (two_peer, x_peer, z))):
                    for wait in waits[:3]:
                        wait.wait_recv()
                    del waits[:3]
                    total = slots[b, 0, part].astype(F32)
                    for o in range(1, RING):
                        total = total + slots[b, o, part].astype(F32)
                    fresh = (old[b, at, part].astype(F32) + total.astype(BF16).astype(F32)).astype(BF16)
                    number = part * RING
                    if b < BLOCKS - 1:
                        old[b + 1, at, part] = fresh
                        place = old.at[b + 1, at, part]
                        peers = ys if half == 0 else zs
                        for o in (2, 1, 3):
                            later.append(send(b, i, 7 + half, number + o, place, place, peers[o - 1]))
                    elif half == 0:
                        final_x[core, y, part, first : first + rows] = fresh
                        place = final_x.at[core, y, part, first : first + rows]
                        for o in (2, 1, 3):
                            later.append(send(b, i, 7, number + o, place, place, ys[o - 1]))
                    else:
                        last_peer[part] = fresh
                        place = final_x.at[core, z, part, first : first + rows]
                        for o in (2, 1, 3, 0):
                            later.append(send(b, i, 8, number + o, last_peer.at[part], place, crossed[o]))
            yield
            for wait in later:
                wait.wait_recv()

    running = [piece_steps(i) for i in range(count)]
    tick = 0
    while running:
        still = []
        for steps in running:
            try:
                next(steps)
                still.append(steps)
            except StopIteration:
                pass
            for _ in range(ADVANCES.get((tick % 5, steps is running[-1]), 0)):
                if waiting:
                    waiting.pop(0)()
        running = still
        tick += 1

    for work in waiting:
        work()
    for copy in counts + swaps + sent:
        copy.wait_send()


def blocks(pieces, *args):
    capacity = sum(rows for _, rows in pieces)
    hbm = pl.BlockSpec(memory_space=pltpu.HBM)
    vmem = pl.BlockSpec(memory_space=pltpu.VMEM)
    scratch = [
        pltpu.VMEM((SHARDS, 1, SEQS), jnp.int32),
        pltpu.VMEM((2 * SEQS, LANES), F32),
        pltpu.VMEM((RING, SHARD_ROWS, 2 * FEATURES), BF16),
        pltpu.VMEM((BLOCKS, FEATURES), F32),
        pltpu.VMEM((BLOCKS, HEADS, 2 * FEATURES, 4 * LANES), BF16),
        pltpu.VMEM((BLOCKS, CHANNELS, 2 * FEATURES), BF16),
        pltpu.VMEM((SEQS, HEADS, LANES, LANES), BF16),
        pltpu.VMEM((RING * max(rows for _, rows in pieces), 2 * FEATURES), BF16),
        pltpu.VMEM((BLOCKS, HEADS, 4, SHARD_ROWS, LANES), F32),
        pltpu.VMEM((HEADS, SHARD_ROWS, LANES), F32),
        pltpu.VMEM((HEADS, SHARD_ROWS, LANES), F32),
        pltpu.VMEM((HEADS, SHARD_ROWS, LANES), F32),
        pltpu.VMEM((BLOCKS, HEADS, SHARD_ROWS, LANES), F32),
        pltpu.VMEM((BLOCKS, HEADS, SHARD_ROWS, LANES), F32),
        pltpu.VMEM((BLOCKS, SEQS, CHANNELS), F32),
        pltpu.SemaphoreType.DMA((24,)),
        pltpu.SemaphoreType.DMA((23,)),
        pltpu.SemaphoreType.DMA((23,)),
        pltpu.SemaphoreType.DMA((SHARDS - 1,)),
        pltpu.SemaphoreType.DMA((SHARDS - 1,)),
        pltpu.SemaphoreType.DMA((BLOCKS, len(pieces), 9, RING * max(HEADS, CHUNKS))),
        pltpu.SemaphoreType.DMA((BLOCKS, len(pieces), 9, RING * max(HEADS, CHUNKS))),
    ]
    for _, rows in pieces:
        scratch += [
            pltpu.VMEM((BLOCKS, RING, CHUNKS, rows, WIDE), BF16),
            pltpu.VMEM((BLOCKS, RING, CHUNKS, rows, WIDE), BF16),
            pltpu.VMEM((BLOCKS, HEADS, RING, rows, 4 * LANES), BF16),
            pltpu.VMEM((BLOCKS, HEADS, RING - 1, rows, 4 * LANES), BF16),
            pltpu.VMEM((BLOCKS, RING, 1, max(rows, LANES)), F32),
            pltpu.VMEM((BLOCKS, RING - 1, 1, max(rows, LANES)), F32),
            pltpu.VMEM((BLOCKS, HEADS, RING, rows, LANES), BF16),
            pltpu.VMEM((BLOCKS, RING, CHUNKS, rows, WIDE), BF16),
            pltpu.VMEM((BLOCKS, RING, CHUNKS, rows, WIDE), BF16),
            pltpu.VMEM((BLOCKS, 2, RING - 1, CHUNKS, rows, WIDE), BF16),
            pltpu.VMEM((BLOCKS, RING, CHUNKS, rows, WIDE), BF16),
            pltpu.VMEM((BLOCKS, RING, CHUNKS, rows, WIDE), BF16),
            pltpu.VMEM((CHUNKS, rows, WIDE), BF16),
        ]
    return pl.pallas_call(
        functools.partial(blocks_kernel, pieces),
        out_shape=(
            jax.ShapeDtypeStruct((2 * SHARDS, 1, SHARD_ROWS), F32),
            jax.ShapeDtypeStruct((1, 1), jnp.int32),
            jax.ShapeDtypeStruct((2, RING, CHUNKS, capacity, WIDE), BF16),
            pltpu.VMEM((BLOCKS, SEQS, HEADS, LANES, LANES), F32),
        ),
        in_specs=[vmem, hbm, vmem] + [hbm] * 4 + [vmem] * 3 + [hbm] * 2,
        out_specs=(vmem, pl.BlockSpec(memory_space=pltpu.SMEM), vmem, vmem),
        scratch_shapes=scratch,
        compiler_params=pltpu.CompilerParams(
            collective_id=len(pieces) + capacity, has_side_effects=True, vmem_limit_bytes=(32 if capacity == CAPACITY else 44) * MIB
        ),
        name="blocks",
    )(*args)


def outputs_kernel(rank, rows, held, act, mixed, states, old, fresh, state_sems, in_sems, out_sems):
    capacity = rows.shape[3]
    shard_rows = [pl.ds(d * SHARD_ROWS, SHARD_ROWS) for d in range(SHARDS)]
    loads = [pltpu.make_async_copy(act.at[shard_rows[d]], old.at[d], in_sems.at[d]) for d in range(SHARDS)]
    for load in loads:
        load.start()
    writes = [pltpu.make_async_copy(held.at[b], states.at[b], state_sems.at[b]) for b in range(BLOCKS)]
    for write in writes:
        write.start()
    for load in loads:
        load.wait()

    def shard(d, carry):
        places = chosen(rank[d], 0, capacity)
        live = dot_rows(places, jnp.ones((capacity, LANES), BF16)) > 0.5
        for chunk in range(CHUNKS):
            spread = dot_rows(places, rows[lax.rem(d, 2), lax.div(d, 2), chunk]).astype(BF16)
            for part in range(WIDE // LANES):
                low = chunk * WIDE + part * LANES
                fresh[d, :, low : low + LANES] = jnp.where(
                    live, spread[:, part * LANES : (part + 1) * LANES], old[d, :, low : low + LANES]
                )
        return carry

    lax.fori_loop(0, SHARDS, shard, 0)
    for d in range(SHARDS):
        write = pltpu.make_async_copy(fresh.at[d], mixed.at[shard_rows[d]], out_sems.at[d])
        write.start()
        writes.append(write)
    for write in writes:
        write.wait()


def write_out(rank, rows, held, act):
    anywhere = pl.BlockSpec(memory_space=pl.ANY)
    vmem = pl.BlockSpec(memory_space=pltpu.VMEM)
    return pl.pallas_call(
        outputs_kernel,
        out_shape=(
            jax.ShapeDtypeStruct(act.shape, BF16),
            jax.ShapeDtypeStruct(held.shape, F32),
        ),
        in_specs=[vmem, vmem, vmem, anywhere],
        out_specs=(anywhere, anywhere),
        scratch_shapes=[
            pltpu.VMEM((SHARDS, SHARD_ROWS, FEATURES), BF16),
            pltpu.VMEM((SHARDS, SHARD_ROWS, FEATURES), BF16),
            pltpu.SemaphoreType.DMA((BLOCKS,)),
            pltpu.SemaphoreType.DMA((SHARDS,)),
            pltpu.SemaphoreType.DMA((SHARDS,)),
        ],
        compiler_params=pltpu.CompilerParams(vmem_limit_bytes=16 * 1024 * 1024),
        name="write_out",
    )(rank, rows, held, act)


CAPACITY = 128
FEW = ((0, 64), (64, 64))
ALL = ((0, 256),)


def local(
    activation_rows,
    fresh_spans,
    entry_rescale_vector,
    probe_kernel,
    retention_kernel,
    content_kernel,
    valve_kernel,
    retention_minimum,
    extra_attenuation,
    channel_rescale_vector,
    emission_kernel,
    memory_grids,
):
    given = (
        fresh_spans.reshape(1, SEQS),
        activation_rows,
        entry_rescale_vector,
        probe_kernel,
        retention_kernel,
        content_kernel,
        valve_kernel,
        retention_minimum,
        jnp.transpose(extra_attenuation, (0, 2, 1)),
        channel_rescale_vector,
        emission_kernel,
        memory_grids,
    )
    rank, many, rows, held = blocks(FEW, *given)
    mixed, states = write_out(rank, rows, held, activation_rows)

    def again(carry):
        rank, _, rows, held = blocks(ALL, *given)
        return (jnp.zeros((), jnp.int32), *write_out(rank, rows, held, activation_rows))

    _, mixed, states = lax.while_loop(lambda carry: carry[0] > 0, again, (many[0, 0], mixed, states))
    return mixed, states


def solution(mesh):
    placed = (
        P(None, "dp"),
        P("dp"),
        P(None, "dp"),
        P(None, "dp", "tp"),
        P(None, "dp", "tp"),
        P(None, "dp", "tp"),
        P(None, "dp", "tp"),
        P(None, "tp"),
        P(None, "dp", "tp"),
        P(None, "tp"),
        P(None, "tp", "dp"),
        P(None, "dp", "tp", None, None),
    )
    return jax.shard_map(
        local,
        mesh=mesh,
        in_specs=placed,
        out_specs=(P(None, "dp"), P(None, "dp", "tp", None, None)),
        check_vma=False,
    )
```

profile of v0, /device:TPU:1, one launch (start us, length us, event | category | flops | bytes accessed | tf_op | source)
XLA Modules:
  0.0 95.2 jit_solution(5503553458736856848)
XLA Ops:
  0.6 0.0 copy-start.1
  0.6 89.4 %blocks.3 = (f32[16,1,256]{2,1,0:T(1,128)S(1)}, s32[1,1]{1,0:T(1,128)}, bf16[2,4,2,128,256]{4,3,2,1,0:T(8,128)(2,1)S(1)}, f32[2,32,2,128,128]{4,3,2,1,0:T(8,128)S(1)}) custom-call(s32[1,32]{1,0:T(1,128)} %bitcast.5, bf16[2048,512]{1,0:T(8,128)(2,1)} %act.1, f32[2,512]{1,0:T(2,128)} %refs_2_.1, bf16[2,512,256]{2,1,0:T(8,128)(2,1)} %refs_3_.1, ...), custom_call_target="tpu_custom_call" | custom-call | tf_op jit(solution)/shard_map/blocks/pallas_call | solution.py:550
  90.0 0.0 copy-start.2
  90.1 0.0 copy-start.3
  90.1 0.0 copy-start.4
  90.1 0.0 copy-start.5
  90.1 0.0 copy-start.6
  90.1 0.0 copy-start.7
  90.1 0.0 copy-start.8
  90.1 0.0 copy-done.1
  90.1 4.2 %write_out.3 = (bf16[2048,512]{1,0:T(8,128)(2,1)}, f32[2,32,2,128,128]{4,3,2,1,0:T(8,128)}) custom-call(f32[16,1,256]{2,1,0:T(1,128)S(1)} %get-tuple-element.89.rank, bf16[2,4,2,128,256]{4,3,2,1,0:T(8,128)(2,1)S(1)} %get-tuple-element.90.rows, f32[2,32,2,128,128]{4,3,2,1,0:T(8,128)S(1)} %get-tuple-element.91.held, bf16[2048,512]{1,0:T(8,128)(2,1)S(1)} %copy-done.1), custom_call_target="tpu_custom_call" | custom-call | tf_op jit(solution)/shard_map/write_out/pallas_call | solution.py:604
  94.3 0.0 copy-done.2
  94.4 0.0 copy-done.3
  94.4 0.0 copy-done.4
  94.4 0.0 copy-done.5
  94.4 0.0 copy-done.6
  94.4 0.0 copy-done.7
  94.4 0.0 copy-done.8
  94.4 0.6 while.11
Async XLA Ops:
  0.6 89.5 %copy-start.1 = (bf16[2048,512]{1,0:T(8,128)(2,1)S(1)}, bf16[2048,512]{1,0:T(8,128)(2,1)}, u32[]{:S(2)}) copy-start(bf16[2048,512]{1,0:T(8,128)(2,1)} %act.1) | copy-start | bytes 6291460
  90.0 4.3 %copy-start.2 = (bf16[2,512,256]{2,1,0:T(8,128)(2,1)S(1)}, bf16[2,512,256]{2,1,0:T(8,128)(2,1)}, u32[]{:S(2)}) copy-start(bf16[2,512,256]{2,1,0:T(8,128)(2,1)} %refs_3_.1) | copy-start | bytes 1572868
  90.1 4.3 %copy-start.3 = (bf16[2,512,256]{2,1,0:T(8,128)(2,1)S(1)}, bf16[2,512,256]{2,1,0:T(8,128)(2,1)}, u32[]{:S(2)}) copy-start(bf16[2,512,256]{2,1,0:T(8,128)(2,1)} %refs_4_.1) | copy-start | bytes 1572868
  90.1 4.3 %copy-start.4 = (f32[2,512]{1,0:T(2,128)S(1)}, f32[2,512]{1,0:T(2,128)}, u32[]{:S(2)}) copy-start(f32[2,512]{1,0:T(2,128)} %refs_2_.1) | copy-start | bytes 12292
  90.1 4.3 %copy-start.5 = (f32[2,256,2]{1,2,0:T(2,128)S(1)}, f32[2,256,2]{1,2,0:T(2,128)}, u32[]{:S(2)}) copy-start(f32[2,256,2]{1,2,0:T(2,128)} %param.22) | copy-start | bytes 12292
  90.1 4.3 %copy-start.6 = (f32[2,256]{1,0:T(2,128)S(1)}, f32[2,256]{1,0:T(2,128)}, u32[]{:S(2)}) copy-start(f32[2,256]{1,0:T(2,128)} %refs_7_.1) | copy-start | bytes 6148
  90.1 4.3 %copy-start.7 = (f32[2,256]{1,0:T(2,128)S(1)}, f32[2,256]{1,0:T(2,128)}, u32[]{:S(2)}) copy-start(f32[2,256]{1,0:T(2,128)} %refs_9_.1) | copy-start | bytes 6148
  90.1 4.3 %copy-start.8 = (s32[32]{0:T(128)S(1)}, s32[32]{0:T(128)}, u32[]{:S(2)}) copy-start(s32[32]{0:T(128)} %param.15) | copy-start | bytes 388
where the time goes:
time: 95.3 us; the launch traced here: 95.2 us
  Pallas kernels  93.6 us (98%)
    pallas_call x1, Pallas kernels, blocks(): pl.pallas_call(functools.partial(blocks_kernel, pieces), out_shape=(jax.S...  89.4 us
    pallas_call x1, Pallas kernels, write_out(): pl.pallas_call(outputs_kernel, out_shape=(jax.ShapeDtypeStruct(act.shape,...  4.2 us

commit v1 on v0

--- a/solution.py
+++ b/solution.py
@@ -246,18 +246,14 @@
         swaps.append(copy)
         return copy
 
-    def send(b, i, phase, number, source, target, peer):
-        copy = pltpu.make_async_remote_copy(
-            source,
-            target,
-            send_sems.at[b, i, phase, number],
-            recv_sems.at[b, i, phase, number],
-            device_id=peer,
-            device_id_type=MESH,
-        )
-        copy.start()
-        sent.append(copy)
-        return copy
+    def scatter(b, i, phase, number, copies, sources, targets):
+        send_sem, recv_sem = send_sems.at[b, i, phase, number], recv_sems.at[b, i, phase, number]
+        for source, target, peer in copies:
+            pltpu.make_async_remote_copy(
+                source, target, send_sem, recv_sem, device_id=peer, device_id_type=MESH
+            ).start()
+        sent.append(pltpu.make_async_copy(sources, sources, send_sem))
+        return pltpu.make_async_copy(targets, targets, recv_sem)
 
     def rows_of(side, j):
         return act.at[pl.ds((j * 2 + side) * SHARD_ROWS, SHARD_ROWS), :]
@@ -321,17 +317,29 @@
         for j in range(RING):
             picked = dot(chosen(rank[j * 2 + core], first, rows), raw[j]).astype(BF16)
             for part in range(CHUNKS):
-                x_own[0, j, part] = picked[:, part * WIDE : (part + 1) * WIDE]
-                x_peer[0, j, part] = picked[:, FEATURES + part * WIDE : FEATURES + (part + 1) * WIDE]
+                x_own[0, part, j] = picked[:, part * WIDE : (part + 1) * WIDE]
+                x_peer[0, part, j] = picked[:, FEATURES + part * WIDE : FEATURES + (part + 1) * WIDE]
         for b in range(BLOCKS):
             wide = max(rows, LANES)
             eye = iota((rows, wide), 0) == iota((rows, wide), 1)
             for j in range(RING):
+                total = jnp.zeros((rows, 1), F32)
+                for part in range(CHUNKS):
+                    own = x_own[b, part, j].astype(F32)
+                    peer = x_peer[b, part, j].astype(F32)
+                    total = total + jnp.sum(own * own + peer * peer, axis=1, keepdims=True)
+                squares[b, j] = jnp.sum(jnp.where(eye, total, 0.0), axis=0, keepdims=True)
+            square_wait = scatter(
+                b, i, 0, 0,
+                [(squares.at[b, around(x, o)], got_squares.at[b, o - 1], xs[o - 1]) for o in (2, 1, 3)],
+                squares.at[b, 0:3], got_squares.at[b],
+            )
+            for j in range(RING):
                 at = slice(j * rows, (j + 1) * rows)
                 for part in range(CHUNKS):
                     low, high = part * WIDE, (part + 1) * WIDE
-                    own = x_own[b, j, part].astype(F32) * gain_in[b : b + 1, low:high]
-                    peer = x_peer[b, j, part].astype(F32) * gain_peer[b : b + 1, low:high]
+                    own = x_own[b, part, j].astype(F32) * gain_in[b : b + 1, low:high]
+                    peer = x_peer[b, part, j].astype(F32) * gain_peer[b : b + 1, low:high]
                     normed[at, low:high] = own.astype(BF16)
                     normed[at, FEATURES + low : FEATURES + high] = peer.astype(BF16)
             waits = []
@@ -349,23 +357,12 @@
                     return carry
 
                 lax.fori_loop(0, 2, project, 0)
-                for o in (2, 1, 3):
-                    waits.append(
-                        send(
-                            b, i, 0, head * RING + o, parts.at[b, head, around(x, o)], got.at[b, head, o - 1], xs[o - 1]
-                        )
+                waits.append(
+                    scatter(
+                        b, i, 1, head,
+                        [(parts.at[b, head, around(x, o)], got.at[b, head, o - 1], xs[o - 1]) for o in (2, 1, 3)],
+                        parts.at[b, head, 0:3], got.at[b, head],
                     )
-            for j in range(RING):
-                total = jnp.zeros((rows, 1), F32)
-                for part in range(CHUNKS):
-                    own = x_own[b, j, part].astype(F32)
-                    peer = x_peer[b, j, part].astype(F32)
-                    total = total + jnp.sum(own * own + peer * peer, axis=1, keepdims=True)
-                squares[b, j] = jnp.sum(jnp.where(eye, total, 0.0), axis=0, keepdims=True)
-            square_waits = []
-            for o in (2, 1, 3):
-                square_waits.append(
-                    send(b, i, 1, o, squares.at[b, around(x, o)], got_squares.at[b, o - 1], xs[o - 1])
                 )
             if i == count - 1:
                 if b == 0:
@@ -374,8 +371,7 @@
                 round_states(b, states, rounded)
             yield
 
-            for wait in square_waits:
-                wait.wait_recv()
+            square_wait.wait()
             square = squares[b, x] + got_squares[b, 0] + got_squares[b, 1] + got_squares[b, 2]
             scale_row = lax.rsqrt(square / D + EPSILON)
             scale = jnp.sum(jnp.where(eye, scale_row, 0.0), axis=1, keepdims=True)
@@ -383,8 +379,7 @@
             picking = chosen(rank[dp], first, rows)
             head_waits = []
             for head in range(HEADS):
-                for wait in waits[head * 3 : head * 3 + 3]:
-                    wait.wait_recv()
+                waits[head].wait()
 
                 for part in range(2):
                     columns = slice(part * CHANNELS, (part + 1) * CHANNELS)
@@ -400,9 +395,10 @@
                 gates(b, head, first, first + rows, (spread, column, minimum, added, q_decayed, own_read, keys, decay_total))
                 reads(b, head, first, (spread, rounded, gain_out, q_decayed, own_read, heads_out))
                 heads[b, head, x] = dot(picking, heads_out[head].astype(BF16)).astype(BF16)
-                for o in (2, 1, 3):
-                    mine = heads.at[b, head, x]
-                    head_waits.append(send(b, i, 2, head * RING + o, mine, mine, xs[o - 1]))
+                mine, three = heads.at[b, head, x], heads.at[b, head, 0:3]
+                head_waits.append(
+                    scatter(b, i, 2, head, [(mine, mine, xs[o - 1]) for o in (2, 1, 3)], three, three)
+                )
             if i == count - 1:
                 for g in range(SEQS // 8):
                     waiting.append(
@@ -414,7 +410,7 @@
             yield
 
             for wait in head_waits:
-                wait.wait_recv()
+                wait.wait()
             all_heads = jnp.concatenate([heads[b, head].reshape(RING * rows, LANES) for head in range(HEADS)], axis=1)
             waits = []
             for part in range(CHUNKS):
@@ -422,14 +418,17 @@
                     low = half * FEATURES + part * WIDE
                     product = dot(all_heads, outward[b, :, low : low + WIDE]).astype(BF16)
                     for j in range(RING):
-                        target[b, j, part] = product[j * rows : (j + 1) * rows]
-                    for o in (2, 1, 3):
-                        waits.append(
-                            send(
-                                b, i, 3 + half, part * RING + o, target.at[b, around(at, o), part],
-                                one.at[b, half, o - 1, part], peers[o - 1],
-                            )
+                        target[b, part, j] = product[j * rows : (j + 1) * rows]
+                    waits.append(
+                        scatter(
+                            b, i, 3 + half, part,
+                            [
+                                (target.at[b, part, around(at, o)], one.at[b, half, part, o - 1], peers[o - 1])
+                                for o in (2, 1, 3)
+                            ],
+                            target.at[b, part, 0:3], one.at[b, half, part],
                         )
+                    )
             yield
 
             later = []
@@ -437,52 +436,49 @@
                 for half, (mine, at, slots, own, peers) in enumerate(
                     ((u_own, y, two_own, z, zs), (u_peer, z, two_peer, y, ys))
                 ):
-                    for wait in waits[:3]:
-                        wait.wait_recv()
-                    del waits[:3]
-                    total = mine[b, at, part].astype(F32)
+                    waits.pop(0).wait()
+                    total = mine[b, part, at].astype(F32)
                     for o in range(RING - 1):
-                        total = total + one[b, half, o, part].astype(F32)
-                    slots[b, own, part] = total.astype(BF16)
-                    place = slots.at[b, own, part]
-                    for o in (2, 1, 3):
-                        later.append(send(b, i, 5 + half, part * RING + o, place, place, peers[o - 1]))
+                        total = total + one[b, half, part, o].astype(F32)
+                    slots[b, part, own] = total.astype(BF16)
+                    place, three = slots.at[b, part, own], slots.at[b, part, 0:3]
+                    later.append(
+                        scatter(b, i, 5 + half, part, [(place, place, peers[o - 1]) for o in (2, 1, 3)], three, three)
+                    )
             waits = later
             yield
 
             later = []
             for part in range(CHUNKS):
                 for half, (slots, old, at) in enumerate(((two_own, x_own, y), (two_peer, x_peer, z))):
-                    for wait in waits[:3]:
-                        wait.wait_recv()
-                    del waits[:3]
-                    total = slots[b, 0, part].astype(F32)
+                    waits.pop(0).wait()
+                    total = slots[b, part, 0].astype(F32)
                     for o in range(1, RING):
-                        total = total + slots[b, o, part].astype(F32)
-                    fresh = (old[b, at, part].astype(F32) + total.astype(BF16).astype(F32)).astype(BF16)
-                    number = part * RING
+                        total = total + slots[b, part, o].astype(F32)
+                    fresh = (old[b, part, at].astype(F32) + total.astype(BF16).astype(F32)).astype(BF16)
+                    within = slice(first, first + rows)
                     if b < BLOCKS - 1:
-                        old[b + 1, at, part] = fresh
-                        place = old.at[b + 1, at, part]
+                        old[b + 1, part, at] = fresh
+                        place, three = old.at[b + 1, part, at], old.at[b + 1, part, 0:3]
                         peers = ys if half == 0 else zs
-                        for o in (2, 1, 3):
-                            later.append(send(b, i, 7 + half, number + o, place, place, peers[o - 1]))
+                        copies = [(place, place, peers[o - 1]) for o in (2, 1, 3)]
+                        later.append(scatter(b, i, 7 + half, part, copies, three, three))
                     elif half == 0:
-                        final_x[core, y, part, first : first + rows] = fresh
-                        place = final_x.at[core, y, part, first : first + rows]
-                        for o in (2, 1, 3):
-                            later.append(send(b, i, 7, number + o, place, place, ys[o - 1]))
+                        final_x[core, part, y, within] = fresh
+                        place, three = final_x.at[core, part, y, within], final_x.at[core, part, 0:3, within]
+                        copies = [(place, place, ys[o - 1]) for o in (2, 1, 3)]
+                        later.append(scatter(b, i, 7, part, copies, three, three))
                     else:
                         last_peer[part] = fresh
-                        place = final_x.at[core, z, part, first : first + rows]
-                        for o in (2, 1, 3, 0):
-                            later.append(send(b, i, 8, number + o, last_peer.at[part], place, crossed[o]))
+                        place, four = final_x.at[core, part, z, within], final_x.at[1 - core, part, 0:4, within]
+                        copies = [(last_peer.at[part], place, crossed[o]) for o in (2, 1, 3, 0)]
+                        later.append(scatter(b, i, 8, part, copies, four, four))
             yield
             for wait in later:
-                wait.wait_recv()
+                wait.wait()
 
     running = [piece_steps(i) for i in range(count)]
-    tick = 0
+    tick, aged = 0, []
     while running:
         still = []
         for steps in running:
@@ -494,13 +490,20 @@
             for _ in range(ADVANCES.get((tick % 5, steps is running[-1]), 0)):
                 if waiting:
                     waiting.pop(0)()
+        for copy in aged:
+            copy.wait()
+        aged = list(sent)
+        sent.clear()
+        if tick == 1:
+            for copy in swaps + counts:
+                copy.wait_send()
         running = still
         tick += 1
 
     for work in waiting:
         work()
-    for copy in counts + swaps + sent:
-        copy.wait_send()
+    for copy in aged + sent:
+        copy.wait()
 
 
 def blocks(pieces, *args):
@@ -528,23 +531,23 @@
         pltpu.SemaphoreType.DMA((23,)),
         pltpu.SemaphoreType.DMA((SHARDS - 1,)),
         pltpu.SemaphoreType.DMA((SHARDS - 1,)),
-        pltpu.SemaphoreType.DMA((BLOCKS, len(pieces), 9, RING * max(HEADS, CHUNKS))),
-        pltpu.SemaphoreType.DMA((BLOCKS, len(pieces), 9, RING * max(HEADS, CHUNKS))),
+        pltpu.SemaphoreType.DMA((BLOCKS, len(pieces), 9, max(HEADS, CHUNKS))),
+        pltpu.SemaphoreType.DMA((BLOCKS, len(pieces), 9, max(HEADS, CHUNKS))),
     ]
     for _, rows in pieces:
         scratch += [
-            pltpu.VMEM((BLOCKS, RING, CHUNKS, rows, WIDE), BF16),
-            pltpu.VMEM((BLOCKS, RING, CHUNKS, rows, WIDE), BF16),
+            pltpu.VMEM((BLOCKS, CHUNKS, RING, rows, WIDE), BF16),
+            pltpu.VMEM((BLOCKS, CHUNKS, RING, rows, WIDE), BF16),
             pltpu.VMEM((BLOCKS, HEADS, RING, rows, 4 * LANES), BF16),
             pltpu.VMEM((BLOCKS, HEADS, RING - 1, rows, 4 * LANES), BF16),
             pltpu.VMEM((BLOCKS, RING, 1, max(rows, LANES)), F32),
             pltpu.VMEM((BLOCKS, RING - 1, 1, max(rows, LANES)), F32),
             pltpu.VMEM((BLOCKS, HEADS, RING, rows, LANES), BF16),
-            pltpu.VMEM((BLOCKS, RING, CHUNKS, rows, WIDE), BF16),
-            pltpu.VMEM((BLOCKS, RING, CHUNKS, rows, WIDE), BF16),
-            pltpu.VMEM((BLOCKS, 2, RING - 1, CHUNKS, rows, WIDE), BF16),
-            pltpu.VMEM((BLOCKS, RING, CHUNKS, rows, WIDE), BF16),
-            pltpu.VMEM((BLOCKS, RING, CHUNKS, rows, WIDE), BF16),
+            pltpu.VMEM((BLOCKS, CHUNKS, RING, rows, WIDE), BF16),
+            pltpu.VMEM((BLOCKS, CHUNKS, RING, rows, WIDE), BF16),
+            pltpu.VMEM((BLOCKS, 2, CHUNKS, RING - 1, rows, WIDE), BF16),
+            pltpu.VMEM((BLOCKS, CHUNKS, RING, rows, WIDE), BF16),
+            pltpu.VMEM((BLOCKS, CHUNKS, RING, rows, WIDE), BF16),
             pltpu.VMEM((CHUNKS, rows, WIDE), BF16),
         ]
     return pl.pallas_call(
@@ -552,7 +555,7 @@
         out_shape=(
             jax.ShapeDtypeStruct((2 * SHARDS, 1, SHARD_ROWS), F32),
             jax.ShapeDtypeStruct((1, 1), jnp.int32),
-            jax.ShapeDtypeStruct((2, RING, CHUNKS, capacity, WIDE), BF16),
+            jax.ShapeDtypeStruct((2, CHUNKS, RING, capacity, WIDE), BF16),
             pltpu.VMEM((BLOCKS, SEQS, HEADS, LANES, LANES), F32),
         ),
         in_specs=[vmem, hbm, vmem] + [hbm] * 4 + [vmem] * 3 + [hbm] * 2,
@@ -581,7 +584,7 @@
         places = chosen(rank[d], 0, capacity)
         live = dot_rows(places, jnp.ones((capacity, LANES), BF16)) > 0.5
         for chunk in range(CHUNKS):
-            spread = dot_rows(places, rows[lax.rem(d, 2), lax.div(d, 2), chunk]).astype(BF16)
+            spread = dot_rows(places, rows[lax.rem(d, 2), chunk, lax.div(d, 2)]).astype(BF16)
             for part in range(WIDE // LANES):
                 low = chunk * WIDE + part * LANES
                 fresh[d, :, low : low + LANES] = jnp.where(

time: 95.3 us -> 88.5 us (0.929)
  Pallas kernels: 93.6 us -> 86.8 us
    pallas_call x1, Pallas kernels: 89.4 us -> 82.6 us  [blocks(): pl.pallas_call(functools.partial(blocks_kernel, pieces), out_shape=(jax.S...]
where the time goes in v1:
time: 88.5 us; the launch traced here: 88.4 us
  Pallas kernels  86.8 us (98%)
  between operations  0.93 us (1%)
    pallas_call x1, Pallas kernels, blocks(): pl.pallas_call(functools.partial(blocks_kernel, pieces), out_shape=(jax.S...  82.6 us
    pallas_call x1, Pallas kernels, write_out(): pl.pallas_call(outputs_kernel, out_shape=(jax.ShapeDtypeStruct(act.shape,...  4.2 us

profile of v1, /device:TPU:1, one launch (start us, length us, event | category | flops | bytes accessed | tf_op | source)
XLA Modules:
  0.0 88.4 jit_solution(13238196486859923700)
XLA Ops:
  0.6 0.0 copy-start.1
  0.6 82.6 %blocks.3 = (f32[16,1,256]{2,1,0:T(1,128)S(1)}, s32[1,1]{1,0:T(1,128)}, bf16[2,2,4,128,256]{4,3,2,1,0:T(8,128)(2,1)S(1)}, f32[2,32,2,128,128]{4,3,2,1,0:T(8,128)S(1)}) custom-call(s32[1,32]{1,0:T(1,128)} %bitcast.5, bf16[2048,512]{1,0:T(8,128)(2,1)} %act.1, f32[2,512]{1,0:T(2,128)} %refs_2_.1, bf16[2,512,256]{2,1,0:T(8,128)(2,1)} %refs_3_.1, ...), custom_call_target="tpu_custom_call" | custom-call | tf_op jit(solution)/shard_map/blocks/pallas_call | solution.py:553
  83.2 0.0 copy-start.2
  83.2 0.0 copy-start.3
  83.2 0.0 copy-start.4
  83.2 0.0 copy-start.5
  83.3 0.0 copy-start.6
  83.3 0.0 copy-start.7
  83.3 0.0 copy-start.8
  83.3 0.0 copy-done.1
  83.3 4.2 %write_out.3 = (bf16[2048,512]{1,0:T(8,128)(2,1)}, f32[2,32,2,128,128]{4,3,2,1,0:T(8,128)}) custom-call(f32[16,1,256]{2,1,0:T(1,128)S(1)} %get-tuple-element.89.rank, bf16[2,2,4,128,256]{4,3,2,1,0:T(8,128)(2,1)S(1)} %get-tuple-element.90.rows, f32[2,32,2,128,128]{4,3,2,1,0:T(8,128)S(1)} %get-tuple-element.91.held, bf16[2048,512]{1,0:T(8,128)(2,1)S(1)} %copy-done.1), custom_call_target="tpu_custom_call" | custom-call | tf_op jit(solution)/shard_map/write_out/pallas_call | solution.py:607
  87.5 0.0 copy-done.2
  87.5 0.0 copy-done.3
  87.5 0.0 copy-done.4
  87.5 0.0 copy-done.5
  87.6 0.0 copy-done.6
  87.6 0.0 copy-done.7
  87.6 0.0 copy-done.8
  87.6 0.6 while.11
Async XLA Ops:
  0.6 82.7 %copy-start.1 = (bf16[2048,512]{1,0:T(8,128)(2,1)S(1)}, bf16[2048,512]{1,0:T(8,128)(2,1)}, u32[]{:S(2)}) copy-start(bf16[2048,512]{1,0:T(8,128)(2,1)} %act.1) | copy-start | bytes 6291460
  83.2 4.3 %copy-start.2 = (bf16[2,512,256]{2,1,0:T(8,128)(2,1)S(1)}, bf16[2,512,256]{2,1,0:T(8,128)(2,1)}, u32[]{:S(2)}) copy-start(bf16[2,512,256]{2,1,0:T(8,128)(2,1)} %refs_3_.1) | copy-start | bytes 1572868
  83.2 4.3 %copy-start.3 = (bf16[2,512,256]{2,1,0:T(8,128)(2,1)S(1)}, bf16[2,512,256]{2,1,0:T(8,128)(2,1)}, u32[]{:S(2)}) copy-start(bf16[2,512,256]{2,1,0:T(8,128)(2,1)} %refs_4_.1) | copy-start | bytes 1572868
  83.2 4.3 %copy-start.4 = (f32[2,512]{1,0:T(2,128)S(1)}, f32[2,512]{1,0:T(2,128)}, u32[]{:S(2)}) copy-start(f32[2,512]{1,0:T(2,128)} %refs_2_.1) | copy-start | bytes 12292
  83.2 4.3 %copy-start.5 = (f32[2,256,2]{1,2,0:T(2,128)S(1)}, f32[2,256,2]{1,2,0:T(2,128)}, u32[]{:S(2)}) copy-start(f32[2,256,2]{1,2,0:T(2,128)} %param.22) | copy-start | bytes 12292
  83.3 4.3 %copy-start.6 = (f32[2,256]{1,0:T(2,128)S(1)}, f32[2,256]{1,0:T(2,128)}, u32[]{:S(2)}) copy-start(f32[2,256]{1,0:T(2,128)} %refs_7_.1) | copy-start | bytes 6148
  83.3 4.3 %copy-start.7 = (f32[2,256]{1,0:T(2,128)S(1)}, f32[2,256]{1,0:T(2,128)}, u32[]{:S(2)}) copy-start(f32[2,256]{1,0:T(2,128)} %refs_9_.1) | copy-start | bytes 6148
  83.3 4.3 %copy-start.8 = (s32[32]{0:T(128)S(1)}, s32[32]{0:T(128)}, u32[]{:S(2)}) copy-start(s32[32]{0:T(128)} %param.15) | copy-start | bytes 388

commit v2 on v1

--- a/solution.py
+++ b/solution.py
@@ -226,25 +226,21 @@
 
     local, swaps, sent = [], [], []
 
-    def bring(source, target):
-        copy = pltpu.make_async_copy(source, target, local_sems.at[len(local)])
-        copy.start()
-        local.append(copy)
-        return copy
-
-    def swap(source, target):
-        number = len(swaps)
-        copy = pltpu.make_async_remote_copy(
-            source,
-            target,
-            swap_send.at[number],
-            swap_recv.at[number],
-            device_id=partner,
-            device_id_type=MESH,
-        )
-        copy.start()
-        swaps.append(copy)
-        return copy
+    def bring(parts, whole):
+        sem = local_sems.at[len(local)]
+        for source, target in parts:
+            pltpu.make_async_copy(source, target, sem).start()
+        local.append(pltpu.make_async_copy(whole, whole, sem))
+        return local[-1]
+
+    def swap(parts, whole):
+        send_sem, recv_sem = swap_send.at[len(swaps)], swap_recv.at[len(swaps)]
+        for source, target in parts:
+            pltpu.make_async_remote_copy(
+                source, target, send_sem, recv_sem, device_id=partner, device_id_type=MESH
+            ).start()
+        swaps.append(pltpu.make_async_copy(whole, whole, send_sem))
+        return pltpu.make_async_copy(whole, whole, recv_sem)
 
     def scatter(b, i, phase, number, copies, sources, targets):
         send_sem, recv_sem = send_sems.at[b, i, phase, number], recv_sems.at[b, i, phase, number]
@@ -258,18 +254,27 @@
     def rows_of(side, j):
         return act.at[pl.ds((j * 2 + side) * SHARD_ROWS, SHARD_ROWS), :]
 
-    def weight_parts(b, head, first):
-        for k in range(4):
-            yield (
+    def row_parts(side, low):
+        columns = slice(low, low + FEATURES)
+        return [(rows_of(side, j), raw.at[j, :, columns]) for j in range(RING)], raw.at[:, :, columns]
+
+    def weight_parts(b, head, low):
+        rows = slice(low, low + FEATURES)
+        parts = [
+            (
                 kernels[k].at[b, :, head * LANES : (head + 1) * LANES],
-                weights.at[b, head, first : first + FEATURES, k * LANES : (k + 1) * LANES],
+                weights.at[b, head, rows, k * LANES : (k + 1) * LANES],
             )
-
-    own_rows = [bring(rows_of(core, j), raw.at[j, :, 0:FEATURES]) for j in range(RING)]
-    own_weights = [[[bring(*part) for part in weight_parts(0, h, 0)] for h in range(HEADS)]]
-    own_states = [bring(memory.at[b], states.at[b]) for b in range(BLOCKS)]
-    own_outward = [bring(emission.at[b], outward.at[b, :, 0:FEATURES]) for b in range(BLOCKS)]
-    own_weights.append([[bring(*part) for part in weight_parts(1, h, 0)] for h in range(HEADS)])
+            for k in range(4)
+        ]
+        return parts, weights.at[b, head, rows]
+
+    def outward_parts(b, low):
+        place = outward.at[b, :, low : low + FEATURES]
+        return [(emission.at[b], place)], place
+
+    own_rows = bring(*row_parts(core, 0))
+    own_weights = [[bring(*weight_parts(0, head, 0)) for head in range(HEADS)]]
 
     greet(xs + ys + zs + crossed + others)
 
@@ -285,21 +290,23 @@
         )
         copy.start()
         counts.append(copy)
-    peer_rows = [swap(rows_of(1 - core, j), raw.at[j, :, FEATURES : 2 * FEATURES]) for j in range(RING)]
-    peer_gain = swap(gain_in, gain_peer)
-    peer_weights = [[[swap(*part) for part in weight_parts(0, h, FEATURES)] for h in range(HEADS)]]
-    peer_outward = [swap(emission.at[b], outward.at[b, :, FEATURES : 2 * FEATURES]) for b in range(BLOCKS)]
-    peer_weights.append([[swap(*part) for part in weight_parts(1, h, FEATURES)] for h in range(HEADS)])
+    peer_rows = swap(*row_parts(1 - core, FEATURES))
+    peer_gain = swap([(gain_in, gain_peer)], gain_peer)
+    peer_weights = [[swap(*weight_parts(0, head, FEATURES)) for head in range(HEADS)]]
+    own_states = [bring([(memory.at[b], states.at[b])], states.at[b]) for b in range(BLOCKS)]
+    own_outward = [bring(*outward_parts(b, 0)) for b in range(BLOCKS)]
+    own_weights.append([bring(*weight_parts(1, head, 0)) for head in range(HEADS)])
+    peer_outward = [swap(*outward_parts(b, FEATURES)) for b in range(BLOCKS)]
+    peer_weights.append([swap(*weight_parts(1, head, FEATURES)) for head in range(HEADS)])
 
     gathered[dp] = spans[...]
     fill_columns(spans, column)
     for copy in counts:
         copy.wait_recv()
     fill_ranks(gathered, rank, many)
-    for j in range(RING):
-        own_rows[j].wait()
-        peer_rows[j].wait_recv()
-    peer_gain.wait_recv()
+    own_rows.wait()
+    peer_rows.wait()
+    peer_gain.wait()
     waiting = []
 
     def widen():
@@ -345,9 +352,8 @@
             waits = []
             for head in range(HEADS):
                 if i == 0:
-                    for k in range(4):
-                        own_weights[b][head][k].wait()
-                        peer_weights[b][head][k].wait_recv()
+                    own_weights[b][head].wait()
+                    peer_weights[b][head].wait()
 
                 def project(k, carry, b=b, head=head):
                     columns = pl.ds(pl.multiple_of(k * CHANNELS, CHANNELS), CHANNELS)
@@ -406,7 +412,7 @@
                     )
             if i == 0:
                 own_outward[b].wait()
-                peer_outward[b].wait_recv()
+                peer_outward[b].wait()
             yield
 
             for wait in head_waits:
@@ -495,7 +501,9 @@
         aged = list(sent)
         sent.clear()
         if tick == 1:
-            for copy in swaps + counts:
+            for copy in swaps:
+                copy.wait()
+            for copy in counts:
                 copy.wait_send()
         running = still
         tick += 1
@@ -526,9 +534,9 @@
         pltpu.VMEM((BLOCKS, HEADS, SHARD_ROWS, LANES), F32),
         pltpu.VMEM((BLOCKS, HEADS, SHARD_ROWS, LANES), F32),
         pltpu.VMEM((BLOCKS, SEQS, CHANNELS), F32),
-        pltpu.SemaphoreType.DMA((24,)),
-        pltpu.SemaphoreType.DMA((23,)),
-        pltpu.SemaphoreType.DMA((23,)),
+        pltpu.SemaphoreType.DMA((9,)),
+        pltpu.SemaphoreType.DMA((8,)),
+        pltpu.SemaphoreType.DMA((8,)),
         pltpu.SemaphoreType.DMA((SHARDS - 1,)),
         pltpu.SemaphoreType.DMA((SHARDS - 1,)),
         pltpu.SemaphoreType.DMA((BLOCKS, len(pieces), 9, max(HEADS, CHUNKS))),
@@ -577,6 +585,10 @@
     writes = [pltpu.make_async_copy(held.at[b], states.at[b], state_sems.at[b]) for b in range(BLOCKS)]
     for write in writes:
         write.start()
+    def write_rows(d):
+        place = mixed.at[pl.ds(pl.multiple_of(d * SHARD_ROWS, SHARD_ROWS), SHARD_ROWS)]
+        return pltpu.make_async_copy(fresh.at[d], place, out_sems.at[d])
+
     for load in loads:
         load.wait()
 
@@ -590,13 +602,12 @@
                 fresh[d, :, low : low + LANES] = jnp.where(
                     live, spread[:, part * LANES : (part + 1) * LANES], old[d, :, low : low + LANES]
                 )
+        write_rows(d).start()
         return carry
 
     lax.fori_loop(0, SHARDS, shard, 0)
     for d in range(SHARDS):
-        write = pltpu.make_async_copy(fresh.at[d], mixed.at[shard_rows[d]], out_sems.at[d])
-        write.start()
-        writes.append(write)
+        write_rows(d).wait()
     for write in writes:
         write.wait()
 

time: 88.5 us -> 87.9 us (level)
  no operation moved by 1% of the time
where the time goes in v2:
time: 87.9 us; the launch traced here: 87.8 us
  Pallas kernels  86.2 us (98%)
  between operations  0.93 us (1%)
    pallas_call x1, Pallas kernels, blocks(): pl.pallas_call(functools.partial(blocks_kernel, pieces), out_shape=(jax.S...  82 us
    pallas_call x1, Pallas kernels, write_out(): pl.pallas_call(outputs_kernel, out_shape=(jax.ShapeDtypeStruct(act.shape,...  4.2 us

profile of v2, /device:TPU:1, one launch (start us, length us, event | category | flops | bytes accessed | tf_op | source)
XLA Modules:
  0.0 87.8 jit_solution(13684852471853302220)
XLA Ops:
  0.6 0.0 copy-start.1
  0.6 82.0 %blocks.3 = (f32[16,1,256]{2,1,0:T(1,128)S(1)}, s32[1,1]{1,0:T(1,128)}, bf16[2,2,4,128,256]{4,3,2,1,0:T(8,128)(2,1)S(1)}, f32[2,32,2,128,128]{4,3,2,1,0:T(8,128)S(1)}) custom-call(s32[1,32]{1,0:T(1,128)} %bitcast.5, bf16[2048,512]{1,0:T(8,128)(2,1)} %act.1, f32[2,512]{1,0:T(2,128)} %refs_2_.1, bf16[2,512,256]{2,1,0:T(8,128)(2,1)} %refs_3_.1, ...), custom_call_target="tpu_custom_call" | custom-call | tf_op jit(solution)/shard_map/blocks/pallas_call | solution.py:561
  82.6 0.0 copy-start.2
  82.6 0.0 copy-start.3
  82.6 0.0 copy-start.4
  82.6 0.0 copy-start.5
  82.7 0.0 copy-start.6
  82.7 0.0 copy-start.7
  82.7 0.0 copy-start.8
  82.7 0.0 copy-done.1
  82.7 4.2 %write_out.3 = (bf16[2048,512]{1,0:T(8,128)(2,1)}, f32[2,32,2,128,128]{4,3,2,1,0:T(8,128)}) custom-call(f32[16,1,256]{2,1,0:T(1,128)S(1)} %get-tuple-element.89.rank, bf16[2,2,4,128,256]{4,3,2,1,0:T(8,128)(2,1)S(1)} %get-tuple-element.90.rows, f32[2,32,2,128,128]{4,3,2,1,0:T(8,128)S(1)} %get-tuple-element.91.held, bf16[2048,512]{1,0:T(8,128)(2,1)S(1)} %copy-done.1), custom_call_target="tpu_custom_call" | custom-call | tf_op jit(solution)/shard_map/write_out/pallas_call | solution.py:618
  86.9 0.0 copy-done.2
  86.9 0.0 copy-done.3
  86.9 0.0 copy-done.4
  86.9 0.0 copy-done.5
  87.0 0.0 copy-done.6
  87.0 0.0 copy-done.7
  87.0 0.0 copy-done.8
  87.0 0.6 while.11
Async XLA Ops:
  0.6 82.1 %copy-start.1 = (bf16[2048,512]{1,0:T(8,128)(2,1)S(1)}, bf16[2048,512]{1,0:T(8,128)(2,1)}, u32[]{:S(2)}) copy-start(bf16[2048,512]{1,0:T(8,128)(2,1)} %act.1) | copy-start | bytes 6291460
  82.6 4.3 %copy-start.2 = (bf16[2,512,256]{2,1,0:T(8,128)(2,1)S(1)}, bf16[2,512,256]{2,1,0:T(8,128)(2,1)}, u32[]{:S(2)}) copy-start(bf16[2,512,256]{2,1,0:T(8,128)(2,1)} %refs_3_.1) | copy-start | bytes 1572868
  82.6 4.3 %copy-start.3 = (bf16[2,512,256]{2,1,0:T(8,128)(2,1)S(1)}, bf16[2,512,256]{2,1,0:T(8,128)(2,1)}, u32[]{:S(2)}) copy-start(bf16[2,512,256]{2,1,0:T(8,128)(2,1)} %refs_4_.1) | copy-start | bytes 1572868
  82.6 4.3 %copy-start.4 = (f32[2,512]{1,0:T(2,128)S(1)}, f32[2,512]{1,0:T(2,128)}, u32[]{:S(2)}) copy-start(f32[2,512]{1,0:T(2,128)} %refs_2_.1) | copy-start | bytes 12292
  82.6 4.3 %copy-start.5 = (f32[2,256,2]{1,2,0:T(2,128)S(1)}, f32[2,256,2]{1,2,0:T(2,128)}, u32[]{:S(2)}) copy-start(f32[2,256,2]{1,2,0:T(2,128)} %param.22) | copy-start | bytes 12292
  82.7 4.3 %copy-start.6 = (f32[2,256]{1,0:T(2,128)S(1)}, f32[2,256]{1,0:T(2,128)}, u32[]{:S(2)}) copy-start(f32[2,256]{1,0:T(2,128)} %refs_7_.1) | copy-start | bytes 6148
  82.7 4.3 %copy-start.7 = (f32[2,256]{1,0:T(2,128)S(1)}, f32[2,256]{1,0:T(2,128)}, u32[]{:S(2)}) copy-start(f32[2,256]{1,0:T(2,128)} %refs_9_.1) | copy-start | bytes 6148
  82.7 4.3 %copy-start.8 = (s32[32]{0:T(128)S(1)}, s32[32]{0:T(128)}, u32[]{:S(2)}) copy-start(s32[32]{0:T(128)} %param.15) | copy-start | bytes 388
